TPU v7x, 32 devices: a whole 2x2x4 slice. The times are simulated.
32 devices in a mesh: sp: 8 (over z, y), tp: 4 (over x, core).
Axes of the slice: x: 2, y: 2, z: 4, core: 2. Of those that a mesh axis runs over, the one named last changes fastest.
Arguments:
- residual: bfloat16 [2048, 2048], P(('sp', 'tp')), may hold values from -6 to 6
- queries: bfloat16 [2048, 2048], P('sp', 'tp'), may hold values from -40 to 40
- key_rows: bfloat16 [2048, 1024], P('sp', 'tp'), may hold values from -40 to 40
- value_rows: bfloat16 [2048, 1024], P('sp', 'tp'), may hold values from -6 to 6
- forget_sums: float32 [2048, 16], P('sp', 'tp'), as said below
- out_weight: bfloat16 [2048, 2048], P('tp'), may hold values from -0.25 to 0.25
- norm_gain: float32 [2048], replicated, may hold values from 0.1 to 1.9
- expert_ids: int32 [2048, 4], P(('sp', 'tp')), may hold values from 0 to 7, all different within a row; in each aligned block of 64 rows (0 to 63, 64 to 127, ...) at most 64 rows name the same one
- route_weights: float32 [2048, 4], P(('sp', 'tp')), may hold values from 0.1 to 1
- expert_gate: bfloat16 [8, 2048, 384], P('sp'), may hold values from -0.125 to 0.125
- expert_up: bfloat16 [8, 2048, 384], P('sp'), may hold values from -0.125 to 0.125
- expert_down: bfloat16 [8, 384, 2048], P('sp'), may hold values from -0.3125 to 0.3125
- shared_gate: bfloat16 [2048, 384], replicated, may hold values from -0.125 to 0.125
- shared_up: bfloat16 [2048, 384], replicated, may hold values from -0.125 to 0.125
- shared_down: bfloat16 [384, 2048], replicated, may hold values from -0.3125 to 0.3125
Outputs:
- layer_out: bfloat16 [2048, 2048], P(('sp', 'tp'))
Inputs may be any that keep to these rules, and one draw needn't show every extreme that they name: `forget_sums`: each head's column never rises from one position to the next. `expert_ids`: each row names 4 different experts; among the rows of one device no expert is named more than 64 times.
All inputs are finite; a program needn't handle non-finite values.
Results may differ from a plain program's by a relative error of at most 0.014.
Values may be sent and summed in bfloat16 or wider, within the bound.
A program may use at most 128 MiB of HBM per device.

v0:
```python
import math

import jax
import jax.numpy as jnp
from jax import lax
from jax.sharding import PartitionSpec as P

HEADS = 16
KV_HEADS = 8
HEAD_DIM = 128
TOPK = 4


routed_scale = 2.5
norm_eps = 1e-06


def absorb_group(carried, query_group, shard_piece, sum_piece, score_scale):
    query_heads, query_sums, query_pos, last_pos = query_group
    key_piece, value_piece = shard_piece
    piece_rows = key_piece.shape[0]
    query_count, local_kv, group_size, head_size = query_heads.shape
    key_block = math.gcd(piece_rows, 1024)
    key_heads = key_piece.reshape(piece_rows, local_kv, head_size)
    value_heads = value_piece.reshape(piece_rows, local_kv, head_size)
    key_sums = sum_piece.reshape(piece_rows, local_kv, group_size).transpose(1, 2, 0)

    def update(block_start, held):
        row_max, row_sum, weighted = held
        key_part = lax.dynamic_slice_in_dim(key_heads, block_start, key_block, 0)
        value_part = lax.dynamic_slice_in_dim(value_heads, block_start, key_block, 0)
        sums_part = lax.dynamic_slice_in_dim(key_sums, block_start, key_block, 2)
        scores = (
            jnp.einsum("qhgd,khd->hgqk", query_heads, key_part, preferred_element_type=jnp.float32)
            * score_scale
        )
        scores = scores + (query_sums[:, :, :, None] - sums_part[:, :, None, :])
        key_pos = block_start + jnp.arange(key_block, dtype=jnp.int32)
        allowed = query_pos[:, None] >= key_pos[None, :]
        scores = jnp.where(allowed, scores, -jnp.inf)
        new_max = jnp.maximum(row_max, jnp.max(scores, axis=3))
        weights = jnp.exp(scores - new_max[:, :, :, None])
        factor = jnp.exp(row_max - new_max)
        row_sum = row_sum * factor + jnp.sum(weights, axis=3)
        products = jnp.einsum(
            "hgqk,khd->qhgd",
            weights.astype(jnp.bfloat16),
            value_part,
            preferred_element_type=jnp.float32,
        )
        weighted = weighted * factor.transpose(2, 0, 1)[:, :, :, None] + products
        return (new_max, row_sum, weighted)

    def one_block(block_index, held):
        block_start = block_index * key_block
        needed = block_start <= last_pos
        return lax.cond(needed, lambda inner: update(block_start, inner), lambda inner: inner, held)

    return lax.fori_loop(0, piece_rows // key_block, one_block, carried)


def finish(carried):
    row_max, row_sum, weighted = carried
    mixed = weighted / row_sum.transpose(2, 0, 1)[:, :, :, None]
    return mixed.reshape(mixed.shape[0], -1).astype(jnp.bfloat16)


def local(
    residual,
    queries,
    key_rows,
    value_rows,
    forget_sums,
    out_weight,
    norm_gain,
    expert_ids,
    route_weights,
    expert_gate,
    expert_up,
    expert_down,
    shared_gate,
    shared_up,
    shared_down,
):
    sp_count = lax.axis_size("sp")
    sp_index = lax.axis_index("sp")
    local_rows = queries.shape[0]
    local_kv = key_rows.shape[1] // HEAD_DIM
    group_size = HEADS // KV_HEADS
    score_scale = HEAD_DIM ** (-0.5)
    own_first = sp_index * local_rows
    all_sums = lax.all_gather(forget_sums, "sp", axis=0, tiled=True)
    positions = own_first + jnp.arange(local_rows, dtype=jnp.int32)
    groups = [
        (
            queries.reshape(queries.shape[0], local_kv, group_size, HEAD_DIM),
            forget_sums.reshape(forget_sums.shape[0], local_kv, group_size).transpose(1, 2, 0),
            positions,
            positions[-1],
        )
    ]

    def initial(query_count):
        return (
            jnp.full((local_kv, group_size, query_count), -1e30, jnp.float32),
            jnp.zeros((local_kv, group_size, query_count), jnp.float32),
            jnp.zeros((query_count, local_kv, group_size, HEAD_DIM), jnp.float32),
        )

    def absorb(states, shard_piece):
        return tuple(
            (
                absorb_group(held, query_group, shard_piece, all_sums, score_scale)
                for held, query_group in zip(states, groups)
            )
        )

    start_states = tuple((initial(query_group[0].shape[0]) for query_group in groups))
    states = absorb(
        start_states,
        (
            lax.all_gather(key_rows, "sp", axis=0, tiled=True),
            lax.all_gather(value_rows, "sp", axis=0, tiled=True),
        ),
    )
    outputs = [finish(held) for held in states]
    attended = outputs[0]
    rows_out = local_rows // lax.axis_size("tp")
    branch = lax.psum_scatter(
        jnp.dot(attended, out_weight, preferred_element_type=jnp.float32).astype(jnp.bfloat16),
        "tp",
        scatter_dimension=0,
        tiled=True,
    ).astype(jnp.float32)
    stream = (residual.astype(jnp.float32) + branch).astype(jnp.bfloat16)
    wide = lax.optimization_barrier(stream).astype(jnp.float32)
    normed = (
        wide * lax.rsqrt(jnp.mean(wide * wide, axis=1, keepdims=True) + norm_eps) * norm_gain
    ).astype(jnp.bfloat16)
    width = normed.shape[1]
    experts_here = expert_gate.shape[0]
    total_experts = experts_here * sp_count
    capacity = 2 * rows_out * TOPK // total_experts
    flat_ids = expert_ids.reshape(-1)
    assigned = flat_ids.shape[0]
    onehot = (flat_ids[:, None] == jnp.arange(total_experts, dtype=jnp.int32)[None, :]).astype(
        jnp.int32
    )
    slot_rank = jnp.sum((jnp.cumsum(onehot, axis=0) - 1) * onehot, axis=1)
    target = flat_ids * capacity + slot_rank
    slot_count = total_experts * capacity
    source = (
        jnp.full((slot_count,), assigned, jnp.int32)
        .at[target]
        .set(jnp.arange(assigned, dtype=jnp.int32))
    )
    padded = jnp.concatenate([normed, jnp.zeros((1, width), jnp.bfloat16)], axis=0)
    outgoing = padded[source // TOPK].reshape(sp_count, experts_here, capacity, width)
    arrived = lax.all_to_all(outgoing, "sp", split_axis=0, concat_axis=0, tiled=True)
    gate_part = jnp.einsum(
        "necd,edf->necf", arrived, expert_gate, preferred_element_type=jnp.float32
    )
    up_part = jnp.einsum("necd,edf->necf", arrived, expert_up, preferred_element_type=jnp.float32)
    hidden = (jax.nn.silu(gate_part) * up_part).astype(jnp.bfloat16)
    processed = jnp.einsum(
        "necf,efd->necd", hidden, expert_down, preferred_element_type=jnp.float32
    ).astype(jnp.bfloat16)
    returned = lax.all_to_all(processed, "sp", split_axis=0, concat_axis=0, tiled=True)
    results = returned.reshape(slot_count, width)
    picked = results[target].reshape(rows_out, TOPK, width).astype(jnp.float32)
    gates = route_weights / jnp.sum(route_weights, axis=1, keepdims=True) * routed_scale
    routed = jnp.sum(gates[:, :, None] * picked, axis=1)
    shared_hidden = (
        jax.nn.silu(jnp.dot(normed, shared_gate, preferred_element_type=jnp.float32))
        * jnp.dot(normed, shared_up, preferred_element_type=jnp.float32)
    ).astype(jnp.bfloat16)
    shared_out = jnp.dot(shared_hidden, shared_down, preferred_element_type=jnp.float32)
    return (wide + shared_out + routed).astype(jnp.bfloat16)


def solution(mesh):
    in_specs = (
        P(("sp", "tp"), None),
        P("sp", "tp"),
        P("sp", "tp"),
        P("sp", "tp"),
        P("sp", "tp"),
        P("tp", None),
        P(),
        P(("sp", "tp"), None),
        P(("sp", "tp"), None),
        P("sp", None, None),
        P("sp", None, None),
        P("sp", None, None),
        P(),
        P(),
        P(),
    )
    out_specs = P(("sp", "tp"), None)
    return jax.shard_map(local, mesh=mesh, in_specs=in_specs, out_specs=out_specs, check_vma=False)
```

profile of v0, /device:TPU:0, one launch (start us, length us, event | category | flops | bytes accessed | tf_op | source)
XLA Modules:
  0.0 271.7 jit_solution(16404299911886271078)
XLA Ops:
  6.5 1.8 copy.30
  8.4 0.0 all-gather.3.cloned.1.call-update
  8.4 0.0 all-gather.5.cloned.1.call-start
  8.4 0.7 all-gather.5.cloned.1.call-update
  9.1 0.0 reduce-scatter.2.cloned.1.call-start
  9.2 0.6 slice.9
  9.8 1.1 copy.31
  10.9 0.2 copy.34
  11.1 0.7 reshape.117
  11.8 33.0 %all_gather.10 = f32[2048,4]{0,1:T(4,128)S(1)} all-gather(f32[256,4]{0,1:T(4,128)} %param.23), channel_id=1, replica_groups=mesh['sp'=8,'tp'=4] {'sp'}, dimensions={0}, use_global_device_ids=true | all-gather | bytes 36864 | tf_op jit(solution)/shard_map/all_gather | solution.py:92
  44.8 6.7 %all-gather.3.cloned.1.call-done = bf16[2048,256]{0,1:T(8,128)(2,1)} async-done(((bf16[256,256]{0,1:T(8,128)(2,1)}), bf16[2048,256]{0,1:T(8,128)(2,1)}) %all-gather.3.cloned.1.call-update) | async-done | bytes 1048592 | tf_op jit(solution)/shard_map/all_gather | solution.py:122
  51.5 2.3 copy.33
  53.8 39.2 %all-gather.5.cloned.1.call-done = bf16[2048,256]{1,0:T(8,128)(2,1)} async-done(((bf16[256,256]{1,0:T(8,128)(2,1)}), bf16[2048,256]{1,0:T(8,128)(2,1)}) %all-gather.5.cloned.1.call-update) | async-done | bytes 1048592 | tf_op jit(solution)/shard_map/all_gather | solution.py:123
  93.0 2.3 copy.32
  95.3 7.0 %while.18 = (s32[]{:T(128)}, f32[2,2,256]{2,1,0:T(2,128)S(1)}, f32[2,2,256]{2,1,0:T(2,128)S(1)}, f32[256,2,2,128]{0,3,2,1:T(8,128)S(1)}, s32[]{:T(128)}, /*index...) while((s32[]{:T(128)}, f32[2,2,256]{2,1,0:T(2,128)S(1)}, ...), condition=%wide.region_5.6_spmd.clone, body=%wide.region_0.5_spmd.clone.sunk | while | flops 555225344 | bytes 20357496 | solution.py:59
  96.0 5.7 %conditional.3 = ((f32[2,2,256]{2,1,0:T(2,128)S(1)}, f32[2,2,256]{2,1,0:T(2,128)S(1)}, f32[256,2,2,128]{0,3,2,1:T(8,128)S(1)})) conditional(s32[]{:T(128)} %convert_element_type.127, (f32[2,2,256]{2,1,0:T(2,128)S(1)}, f32[2,2,256]{2,1,0:T(2,128)S(1)}, f32[256,2,2,128]{0,3,2,1:T(8,128)S(1)}) %tuple.46, (s32[]{:T(128)}, s32[]{:T(128)}, ...), branch_computations={%region_1.0_spmd, %region_2.4_spmd} | conditional | flops 555225344 | bytes 20356210 | solution.py:57
  96.0 0.2 broadcast_compare_fusion
  96.3 2.3 fusion.5
  98.6 1.6 fusion.12
  100.2 1.4 fusion.4
  102.4 1.7 convolution_convert_fusion.1
  104.1 0.0 reduce-scatter.2.cloned.1.call-update
  104.2 0.1 copy.37
  104.3 0.1 eq.29
  104.4 0.1 eq.25
  104.5 0.6 reduce-window.6
  105.1 0.2 slice_reduce_fusion
  105.4 0.1 copy.36
  105.5 0.1 mul.106
  105.6 0.1 fusion.75
  105.7 1.4 scatter_custom_fusion
  107.1 26.4 %reduce-scatter.2.cloned.1.call-done = bf16[64,2048]{1,0:T(8,128)(2,1)} async-done(((bf16[256,2048]{1,0:T(8,128)(2,1)}), bf16[64,2048]{1,0:T(8,128)(2,1)}) %reduce-scatter.2.cloned.1.call-update) | async-done | bytes 262160 | tf_op jit(solution)/shard_map/reduce_scatter | solution.py:129
  133.5 1.0 add_convert_fusion
  134.5 0.2 fusion.65
  134.7 0.1 fusion.67
  134.9 3.3 %gather_fusion = bf16[512,2048]{1,0:T(8,128)(2,1)} fusion(bf16[65,2048]{1,0:T(8,128)(2,1)S(1)} %concatenate.3, s32[1024]{0:T(1024)S(1)} %pad_clamp_fusion.1), kind=kCustom, calls=%fused_computation | custom fusion | bytes 4196352 | tf_op jit(solution)/shard_map/gather | solution.py:158
  138.2 53.7 %all_to_all.10 = bf16[8,1,64,2048]{3,2,1,0:T(8,128)(2,1)S(1)} all-to-all(bf16[8,1,64,2048]{3,2,1,0:T(8,128)(2,1)} %bitcast.136), channel_id=1, replica_groups=mesh['sp'=8,'tp'=4] {'sp'}, dimensions={0} | all-to-all | bytes 4194304 | tf_op jit(solution)/shard_map/all_to_all | solution.py:159
  192.0 1.3 copy-done.1
  193.2 1.2 fusion.35
  194.5 6.2 %fusion.25 = bf16[8,1,64,2048]{3,2,1,0:T(8,128)(2,1)} fusion(bf16[1,384,2048]{2,1,0:T(8,128)(2,1)} %param.30, bf16[1,2048,384]{2,1,0:T(8,128)(2,1)} %param.29, bf16[8,1,64,2048]{3,2,1,0:T(8,128)(2,1)} %copy-done.1, f32[8,1,64,384]{3,2,0,1:T(8,128)S(1)} %fusion.35), kind=kOutput, calls=%fused_computation.31 | convolution fusion | flops 1612840960 | bytes 8126464 | tf_op jit(solution)/shard_map/necf,efd->necd/dot_general | solution.py:165
  200.7 4.7 %all-to-all-start.1 = ((bf16[8,1,64,2048]{3,2,1,0:T(8,128)(2,1)}), bf16[8,1,64,2048]{3,2,1,0:T(8,128)(2,1)}, u32[]{:S(2)}, u32[]{:S(2)}) async-start(bf16[8,1,64,2048]{3,2,1,0:T(8,128)(2,1)} %fusion.25), calls=%async_computation.2 | async-start | bytes 4194304 | tf_op jit(solution)/shard_map/all_to_all | solution.py:168
  205.5 0.1 copy.35
  205.6 1.8 fusion.85
  207.4 45.2 %all-to-all-done.1 = bf16[8,1,64,2048]{3,2,1,0:T(8,128)(2,1)} async-done(((bf16[8,1,64,2048]{3,2,1,0:T(8,128)(2,1)}), bf16[8,1,64,2048]{3,2,1,0:T(8,128)(2,1)}, u32[]{:S(2)}, u32[]{:S(2)}) %all-to-all-start.1) | async-done | bytes 2097184 | tf_op jit(solution)/shard_map/all_to_all | solution.py:168
  252.6 4.2 %gather_fusion.1 = bf16[256,2048]{1,0:T(8,128)(2,1)S(1)} fusion(bf16[512,2048]{1,0:T(8,128)(2,1)} %bitcast.41, s32[1024]{0:T(1024)S(1)} %pad_clamp_fusion), kind=kCustom, calls=%fused_computation.1 | custom fusion | bytes 2098176 | tf_op jit(solution)/shard_map/gather | solution.py:170
  256.8 1.7 reshape.128
  258.5 3.2 %multiply_reduce_fusion = f32[64,2048]{1,0:T(8,128)S(1)} fusion(f32[64,4,2048]{2,1,0:T(4,128)} %reshape.128, f32[64,4]{1,0:T(8,128)S(1)} %copy.35), kind=kLoop, calls=%fused_computation.40 | loop fusion | flops 917504 | bytes 2622464 | tf_op jit(solution)/shard_map/reduce_sum | solution.py:172
  261.7 3.4 %fusion.27 = bf16[64,2048]{1,0:T(8,128)(2,1)} fusion(f32[64,2048]{1,0:T(8,128)S(1)} %multiply_reduce_fusion, bf16[384,2048]{1,0:T(8,128)(2,1)} %param.33, bf16[2048,384]{1,0:T(8,128)(2,1)} %param.32, bf16[64,2048]{1,0:T(8,128)(2,1)S(1)} %add_convert_fusion, f32[64,384]{1,0:T(8,128)S(1)} %fusion.85, f32[2048]{0:T(1024)S(1)} %copy-done.4, ...), kind=kOutput, calls=%fused_computation.35 | convolution fusion | flops 202522624 | bytes 4301056 | tf_op jit(solution)/shard_map/dot_general | solution.py:177
  (44 shorter events, 0.4 us)
Async XLA Ops:
  6.5 95.8 %copy-start = (bf16[512,2048]{1,0:T(8,128)(2,1)S(1)}, bf16[512,2048]{1,0:T(8,128)(2,1)}, u32[]{:S(2)}) copy-start(bf16[512,2048]{1,0:T(8,128)(2,1)} %param.24) | copy-start | bytes 6291460
  6.5 45.0 %all-gather.3.cloned.1.call-start = ((), (), s32[]{:S(2)}) async-start(), calls=%async_computation.3 | async-start | bytes 1179648 | tf_op jit(solution)/shard_map/all_gather | solution.py:122
  8.4 84.6 %all-gather.5.cloned.1.call-start = ((), (), s32[]{:S(2)}) async-start(), calls=%async_computation.4 | async-start | bytes 1179648 | tf_op jit(solution)/shard_map/all_gather | solution.py:123
  9.1 124.4 %reduce-scatter.2.cloned.1.call-start = ((), (), s32[]{:S(2)}) async-start(), calls=%async_computation.5 | async-start | bytes 1310720 | tf_op jit(solution)/shard_map/reduce_scatter | solution.py:129
  96.2 2.4 copy-start.2
  102.4 1.8 copy-start.5
  102.4 31.1 %copy-start.3 = (bf16[64,2048]{1,0:T(8,128)(2,1)S(1)}, bf16[64,2048]{1,0:T(8,128)(2,1)}, u32[]{:S(2)}) copy-start(bf16[64,2048]{1,0:T(8,128)(2,1)} %param.19) | copy-start | bytes 786436
  102.4 32.3 %copy-start.4 = (f32[2048]{0:T(1024)S(1)}, f32[2048]{0:T(1024)}, u32[]{:S(2)}) copy-start(f32[2048]{0:T(1024)} %param.25) | copy-start | bytes 24580
  138.2 55.0 %copy-start.7 = (bf16[1,2048,384]{2,1,0:T(8,128)(2,1)S(1)}, bf16[1,2048,384]{2,1,0:T(8,128)(2,1)}, u32[]{:S(2)}) copy-start(bf16[1,2048,384]{2,1,0:T(8,128)(2,1)} %param.28) | copy-start | bytes 4718596
  191.9 1.3 copy-start.1
  200.7 4.7 %copy-start.6 = (f32[64,4]{0,1:T(4,128)S(1)}, f32[64,4]{0,1:T(4,128)}, u32[]{:S(2)}) copy-start(f32[64,4]{0,1:T(4,128)} %param.27) | copy-start | bytes 3076
  200.7 51.8 %all-to-all-start.1 = ((bf16[8,1,64,2048]{3,2,1,0:T(8,128)(2,1)}), bf16[8,1,64,2048]{3,2,1,0:T(8,128)(2,1)}, u32[]{:S(2)}, u32[]{:S(2)}) async-start(bf16[8,1,64,2048]{3,2,1,0:T(8,128)(2,1)} %fusion.25), calls=%async_computation.2 | async-start | bytes 4194304 | tf_op jit(solution)/shard_map/all_to_all | solution.py:168
Sparse Core Ops, SparseCore 0:
  9.4 42.1 all-gather.2
  53.7 39.2 all-gather.4
  104.3 29.1 reduce-scatter.1
where the time goes:
time: 272 us
  waiting for transfers between devices  118 us (43%)
  blocking collectives  86.7 us (32%)
  local copies, waits for them, and re-layouts  21.9 us (8%)
  matrix products  18.4 us (7%)
  between operations  13.3 us (5%)
  other arithmetic  6.9 us (3%)
  starting transfers between devices  4.77 us (2%)
    all_to_all x1, blocking collectives, local(): lax.all_to_all(outgoing, 'sp', split_axis=0, concat_axis=0, tiled=True)  53.7 us
    all_to_all x1, waiting for transfers between devices, local(): lax.all_to_all(processed, 'sp', split_axis=0, concat_axis=0, tiled=True)  45.2 us
    all_gather x1, waiting for transfers between devices, local(): lax.all_gather(value_rows, 'sp', axis=0, tiled=True)  39.2 us
    all_gather x1, blocking collectives, local(): all_sums = lax.all_gather(forget_sums, 'sp', axis=0, tiled=True)  33 us
    reduce_scatter x1, waiting for transfers between devices, local(): lax.psum_scatter(jnp.dot(attended, out_weight, preferred_element_type=jnp...  26.4 us
    unnamed x19, local copies, waits for them, and re-layouts  6.76 us
    all_gather x1, waiting for transfers between devices, local(): lax.all_gather(key_rows, 'sp', axis=0, tiled=True)  6.72 us
    dot_general x1, matrix products, local(): jnp.einsum('necf,efd->necd', hidden, expert_down, preferred_element_type=...  6.24 us
  transfers between devices with their start and end apart: 4, of which 4 were waited for; matrix products, arithmetic and copies ran while one was open for 4% of the time, Pallas kernels for 0%

commit v1 on v0

--- a/solution.py
+++ b/solution.py
@@ -1,8 +1,11 @@
+import functools
 import math
 
 import jax
 import jax.numpy as jnp
 from jax import lax
+from jax.experimental import pallas as pl
+from jax.experimental.pallas import tpu as pltpu
 from jax.sharding import PartitionSpec as P
 
 HEADS = 16
@@ -13,6 +16,626 @@
 
 routed_scale = 2.5
 norm_eps = 1e-06
+
+
+MESH_ID = pl.DeviceIdType.MESH
+LOG2E = math.log2(math.e)
+
+
+def remote(src, dst, send_sem, recv_sem, target):
+    return pltpu.make_async_remote_copy(
+        src_ref=src,
+        dst_ref=dst,
+        send_sem=send_sem,
+        recv_sem=recv_sem,
+        device_id=target,
+        device_id_type=MESH_ID,
+    )
+
+
+def greet(barrier, target):
+    pl.semaphore_signal(barrier, inc=1, device_id=target, device_id_type=MESH_ID)
+
+
+def attend_kernel(
+    sp_count,
+    score_scale,
+    q_ref,
+    fq_ref,
+    k_hbm,
+    v_hbm,
+    fk_hbm,
+    out_ref,
+    kbuf,
+    vbuf,
+    fbuf,
+    qs,
+    acc,
+    top,
+    den,
+    load_sem,
+    up_sem,
+    side_sem,
+    recv_sem,
+):
+    me, tp = lax.axis_index("sp"), lax.axis_index("tp")
+    line = sp_count // 2
+    z, y = me // 2, me % 2
+    mate = (2 * z + 1 - y, tp)
+    above = (jnp.minimum(me + 2, sp_count - 1), tp)
+    below = (jnp.maximum(me - 2, 0), tp)
+    bufs = (kbuf, vbuf, fbuf)
+    loads = [
+        pltpu.make_async_copy(src, buf.at[me], load_sem.at[i])
+        for i, (src, buf) in enumerate(zip((k_hbm, v_hbm, fk_hbm), bufs))
+    ]
+    for copy in loads:
+        copy.start()
+    barrier = pltpu.get_barrier_semaphore()
+    greet(barrier, mate)
+
+    @pl.when(z < line - 1)
+    def _():
+        greet(barrier, above)
+
+    @pl.when(z > 0)
+    def _():
+        greet(barrier, below)
+
+    rows, pair = q_ref.shape[0], qs.shape[1] // q_ref.shape[0]
+    kv_heads = qs.shape[0]
+    for h in range(kv_heads * pair):
+        qs[h // pair, (h % pair) * rows : (h % pair + 1) * rows, :] = q_ref[
+            :, h * HEAD_DIM : (h + 1) * HEAD_DIM
+        ]
+    for copy in loads:
+        copy.wait()
+    neighbours = 1 + (z < line - 1).astype(jnp.int32) + (z > 0).astype(jnp.int32)
+    pl.semaphore_wait(barrier, neighbours)
+
+    def moves(block, step, sems, target):
+        return [
+            remote(buf.at[block], buf.at[block], sems.at[step, i], recv_sem.at[block, i], target)
+            for i, buf in enumerate(bufs)
+        ]
+
+    def forward(step):
+        block = 2 * (z - step) + y
+
+        @pl.when(z < line - 1)
+        def _():
+            for copy in moves(block, step, up_sem, above):
+                copy.start()
+
+        @pl.when(jnp.logical_or(y == 0, step > 0))
+        def _():
+            for copy in moves(block, step, side_sem, mate):
+                copy.start()
+
+    def absorb(block, first):
+        for g in range(kv_heads):
+            lanes = slice(g * HEAD_DIM, (g + 1) * HEAD_DIM)
+            keys, values = kbuf[block, :, lanes], vbuf[block, :, lanes]
+            products = lax.dot_general(
+                qs[g], keys, (((1,), (1,)), ((), ())), preferred_element_type=jnp.float32
+            )
+            parts = []
+            for j in range(pair):
+                h = g * pair + j
+                drop = fq_ref[:, h : h + 1] - fbuf[block, h : h + 1, :]
+                part = products[j * rows : (j + 1) * rows] * (score_scale * LOG2E) + drop * LOG2E
+                if first:
+                    at_row = lax.broadcasted_iota(jnp.int32, part.shape, 0)
+                    at_col = lax.broadcasted_iota(jnp.int32, part.shape, 1)
+                    part = jnp.where(at_row >= at_col, part, -jnp.inf)
+                parts.append(part)
+            scores = jnp.concatenate(parts, axis=0)
+            peak = jnp.max(scores, axis=1, keepdims=True)
+            if first:
+                weights = jnp.exp2(scores - peak)
+                total = jnp.sum(weights, axis=1, keepdims=True)
+            else:
+                old = top[g][:, :1]
+                peak = jnp.maximum(old, peak)
+                factor = jnp.exp2(old - peak)
+                weights = jnp.exp2(scores - peak)
+                total = den[g][:, :1] * factor + jnp.sum(weights, axis=1, keepdims=True)
+            mixed = jnp.dot(weights.astype(jnp.bfloat16), values, preferred_element_type=jnp.float32)
+            acc[g] = mixed if first else acc[g] * factor + mixed
+            top[g] = jnp.broadcast_to(peak, top.shape[1:])
+            den[g] = jnp.broadcast_to(total, den.shape[1:])
+
+    forward(0)
+    absorb(me, True)
+
+    def one_step(step, _):
+        @pl.when(step <= z)
+        def _():
+            block = 2 * (z - step) + y
+            for copy in moves(block, step, up_sem, below):
+                copy.wait_recv()
+            forward(step)
+            absorb(block, False)
+
+        @pl.when(jnp.logical_and(step - 1 <= z, jnp.logical_or(y == 1, step > 1)))
+        def _():
+            block = 2 * (z - step + 1) + 1 - y
+            for copy in moves(block, step - 1, side_sem, mate):
+                copy.wait_recv()
+            absorb(block, False)
+
+        return 0
+
+    lax.fori_loop(1, line + 1, one_step, 0)
+    for g in range(kv_heads):
+        done = (acc[g] / den[g]).astype(jnp.bfloat16)
+        for j in range(pair):
+            h = g * pair + j
+            out_ref[:, h * HEAD_DIM : (h + 1) * HEAD_DIM] = done[j * rows : (j + 1) * rows]
+
+    def drain(step, _):
+        @pl.when(step <= z)
+        def _():
+            block = 2 * (z - step) + y
+
+            @pl.when(z < line - 1)
+            def _():
+                for copy in moves(block, step, up_sem, above):
+                    copy.wait_send()
+
+            @pl.when(jnp.logical_or(y == 0, step > 0))
+            def _():
+                for copy in moves(block, step, side_sem, mate):
+                    copy.wait_send()
+
+        return 0
+
+    lax.fori_loop(0, line, drain, 0)
+
+
+def attend_fused(queries, key_rows, value_rows, forget_sums, sp_count):
+    rows, width = queries.shape
+    kv_heads = key_rows.shape[1] // HEAD_DIM
+    heads = width // HEAD_DIM
+    key_sums = jnp.pad(forget_sums.T, ((0, 8 - heads), (0, 0)))
+    line = sp_count // 2
+    stacked = (kv_heads, heads // kv_heads * rows, HEAD_DIM)
+    vmem, hbm = pl.BlockSpec(memory_space=pltpu.VMEM), pl.BlockSpec(memory_space=pl.ANY)
+    return pl.pallas_call(
+        functools.partial(attend_kernel, sp_count, HEAD_DIM ** (-0.5)),
+        out_shape=jax.ShapeDtypeStruct((rows, width), jnp.bfloat16),
+        in_specs=[vmem, vmem, hbm, hbm, hbm],
+        out_specs=vmem,
+        scratch_shapes=[
+            pltpu.VMEM((sp_count,) + key_rows.shape, jnp.bfloat16),
+            pltpu.VMEM((sp_count,) + value_rows.shape, jnp.bfloat16),
+            pltpu.VMEM((sp_count,) + key_sums.shape, jnp.float32),
+            pltpu.VMEM(stacked, jnp.bfloat16),
+            pltpu.VMEM(stacked, jnp.float32),
+            pltpu.VMEM(stacked, jnp.float32),
+            pltpu.VMEM(stacked, jnp.float32),
+            pltpu.SemaphoreType.DMA((3,)),
+            pltpu.SemaphoreType.DMA((line, 3)),
+            pltpu.SemaphoreType.DMA((line, 3)),
+            pltpu.SemaphoreType.DMA((sp_count, 3)),
+        ],
+        compiler_params=pltpu.CompilerParams(
+            collective_id=0, has_side_effects=True, vmem_limit_bytes=60 * 2**20
+        ),
+    )(queries, forget_sums, key_rows, value_rows, key_sums)
+
+
+def tail_kernel(
+    sp_count,
+    att_ref,
+    res_ref,
+    gain_ref,
+    gate_hbm,
+    wo_hbm,
+    eg_hbm,
+    eu_hbm,
+    ed_hbm,
+    sg_hbm,
+    su_hbm,
+    sd_hbm,
+    out_ref,
+    wo,
+    eg,
+    eu,
+    ed,
+    sg,
+    su,
+    sd,
+    gate_in,
+    gate_buf,
+    core_out,
+    core_in,
+    kept,
+    x_out,
+    x_in,
+    base,
+    tok,
+    side_out,
+    side_in,
+    own,
+    up_out,
+    up_in,
+    dn_out,
+    dn_in,
+    load_sem,
+    gsend_sem,
+    grecv_sem,
+    pair_sem,
+    hop_sem,
+    tok_sem,
+    side_send,
+    side_recv,
+    up_send,
+    up_recv,
+    dn_send,
+    dn_recv,
+):
+    me, tp = lax.axis_index("sp"), lax.axis_index("tp")
+    line = sp_count // 2
+    z, y = me // 2, me % 2
+    x, c = tp // 2, tp % 2
+    mate = (2 * z + 1 - y, tp)
+    above = (jnp.minimum(me + 2, sp_count - 1), tp)
+    below = (jnp.maximum(me - 2, 0), tp)
+    core_mate = (me, 2 * x + 1 - c)
+    x_mate = (me, 2 * (1 - x) + c)
+    rows = res_ref.shape[0]
+    weights = [
+        pltpu.make_async_copy(src, dst, load_sem.at[i])
+        for i, (src, dst) in enumerate(
+            (
+                (gate_hbm, gate_in),
+                (wo_hbm, wo),
+                (sg_hbm, sg),
+                (su_hbm, su),
+                (sd_hbm, sd),
+                (eg_hbm, eg),
+                (eu_hbm, eu),
+                (ed_hbm, ed),
+            )
+        )
+    ]
+    for copy in weights:
+        copy.start()
+    barrier = pltpu.get_barrier_semaphore()
+    greet(barrier, core_mate)
+    greet(barrier, x_mate)
+    for j in range(1, sp_count):
+        greet(barrier, (lax.rem(me + j, sp_count), tp))
+    weights[0].wait()
+    weights[1].wait()
+    pl.semaphore_wait(barrier, sp_count + 1)
+
+    def gate_move(j):
+        peer, source = lax.rem(me + j, sp_count), me
+        return remote(
+            gate_in.at[peer], gate_buf.at[source], gsend_sem.at[j - 1], grecv_sem.at[j - 1], (peer, tp)
+        )
+
+    def gate_arrival(j):
+        source = lax.rem(me - j + sp_count, sp_count)
+        return remote(
+            gate_in.at[source], gate_buf.at[source], gsend_sem.at[j - 1], grecv_sem.at[j - 1], (source, tp)
+        )
+
+    for j in range(1, sp_count):
+        gate_move(j).start()
+
+    far, near = (1 - x) * 2, x * 2
+
+    def project(block):
+        return jnp.dot(
+            att_ref[pl.ds(pl.multiple_of(block * rows, rows), rows), :],
+            wo[...],
+            preferred_element_type=jnp.float32,
+        )
+
+    def project_to(i, _):
+        out_x = jnp.where(i % 2 == 0, far, near)
+
+        @pl.when(i < 2)
+        def _():
+            core_out[i % 2] = project(out_x + 1 - c).astype(jnp.bfloat16)
+            remote(
+                core_out.at[i % 2], core_in.at[i % 2], pair_sem.at[0, i % 2], pair_sem.at[1, i % 2], core_mate
+            ).start()
+
+        @pl.when(i >= 2)
+        def _():
+            kept[i % 2] = project(out_x + c)
+
+        return 0
+
+    lax.fori_loop(0, 4, project_to, 0)
+
+    def core_copy(i):
+        return remote(core_out.at[i], core_in.at[i], pair_sem.at[0, i], pair_sem.at[1, i], core_mate)
+
+    core_copy(0).wait_recv()
+    x_out[...] = (kept[0] + core_in[0].astype(jnp.float32)).astype(jnp.bfloat16)
+    hop = remote(x_out, x_in, hop_sem.at[0], hop_sem.at[1], x_mate)
+    hop.start()
+    core_copy(1).wait_recv()
+    branch = kept[1] + core_in[1].astype(jnp.float32) + res_ref[...].astype(jnp.float32)
+    hop.wait_recv()
+    stream = (branch + x_in[...].astype(jnp.float32)).astype(jnp.bfloat16)
+    wide = stream.astype(jnp.float32)
+    scale = lax.rsqrt(jnp.mean(wide * wide, axis=1, keepdims=True) + norm_eps)
+    tok[me] = (wide * scale * gain_ref[...]).astype(jnp.bfloat16)
+    base[...] = wide
+
+    def tok_move(block, sem, target):
+        return remote(tok.at[block], tok.at[block], sem, tok_sem.at[block], target)
+
+    def block_of(where):
+        return 2 * where + y
+
+    def send_up(where):
+        return tok_move(block_of(where), up_send.at[where], above)
+
+    def send_dn(where):
+        return tok_move(block_of(where), dn_send.at[where], below)
+
+    def send_side(where):
+        return tok_move(block_of(where), side_send.at[where], mate)
+
+    send_side(z).start()
+
+    @pl.when(z < line - 1)
+    def _():
+        send_up(z).start()
+
+    @pl.when(z > 0)
+    def _():
+        send_dn(z).start()
+
+    for copy in weights[2:]:
+        copy.wait()
+
+    def gated(inputs, gate, up, down):
+        first = jnp.dot(inputs, gate[...], preferred_element_type=jnp.float32)
+        second = jnp.dot(inputs, up[...], preferred_element_type=jnp.float32)
+        hidden = (first / (1.0 + jnp.exp(-first)) * second).astype(jnp.bfloat16)
+        return jnp.dot(hidden, down[...], preferred_element_type=jnp.float32)
+
+    base[...] += gated(tok[me], sg, su, sd)
+    for j in range(1, sp_count):
+        gate_arrival(j).wait_recv()
+    gate_buf[me] = gate_in[me]
+
+    def expert(block):
+        row = gate_buf[block][:1, :]
+        shape = (rows, row.shape[1])
+        diagonal = lax.broadcasted_iota(jnp.int32, shape, 0) == lax.broadcasted_iota(jnp.int32, shape, 1)
+        column = jnp.sum(jnp.where(diagonal, row, 0.0), axis=1, keepdims=True)
+        result = gated(tok[block], eg, eu, ed).astype(jnp.bfloat16).astype(jnp.float32)
+        return result * column
+
+    def side_back(where):
+        return remote(
+            side_out.at[where], side_in.at[where], side_send.at[line + where], side_recv.at[where], mate
+        )
+
+    def mates_block(where):
+        tok_move(2 * where + 1 - y, side_send.at[where], mate).wait_recv()
+        side_out[where] = expert(2 * where + 1 - y).astype(jnp.bfloat16)
+        side_back(where).start()
+
+    own[z] = expert(me)
+    mates_block(z)
+
+    def one_step(step, _):
+        low, high = z - step, z + step
+
+        @pl.when(low >= 0)
+        def _():
+            tok_move(block_of(low), up_send.at[low], below).wait_recv()
+            send_side(low).start()
+
+            @pl.when(z < line - 1)
+            def _():
+                send_up(low).start()
+
+        @pl.when(high < line)
+        def _():
+            tok_move(block_of(high), dn_send.at[high], above).wait_recv()
+            send_side(high).start()
+
+            @pl.when(z > 0)
+            def _():
+                send_dn(high).start()
+
+        def at(i, _):
+            where = jnp.where(i == 0, low, high)
+
+            @pl.when(jnp.logical_and(where >= 0, where < line))
+            def _():
+                own[where] = expert(block_of(where))
+
+            return 0
+
+        def at_mates(i, _):
+            where = jnp.where(i == 0, low, high)
+
+            @pl.when(jnp.logical_and(where >= 0, where < line))
+            def _():
+                mates_block(where)
+
+            return 0
+
+        lax.fori_loop(0, 2, at, 0)
+        lax.fori_loop(0, 2, at_mates, 0)
+        return 0
+
+    lax.fori_loop(1, line, one_step, 0)
+
+    def up_back(where):
+        return remote(up_out.at[where], up_in.at[where], up_send.at[line + where], up_recv.at[where], above)
+
+    def dn_back(where):
+        return remote(dn_out.at[where], dn_in.at[where], dn_send.at[line + where], dn_recv.at[where], below)
+
+    def back_step(turn, _):
+        step = turn % (line - 1) + 1
+        upward = (turn < line - 1) == (2 * z < line - 1)
+        low, high = z - step, z + step
+
+        @pl.when(jnp.logical_and(upward, high < line))
+        def _():
+            side_back(high).wait_recv()
+            own[high] = own[high] + side_in[high].astype(jnp.float32)
+
+            @pl.when(z > 0)
+            def _():
+                up_back(high).wait_recv()
+                own[high] = own[high] + up_in[high].astype(jnp.float32)
+
+            up_out[high] = own[high].astype(jnp.bfloat16)
+            up_back(high).start()
+
+        @pl.when(jnp.logical_and(jnp.logical_not(upward), low >= 0))
+        def _():
+            side_back(low).wait_recv()
+            own[low] = own[low] + side_in[low].astype(jnp.float32)
+
+            @pl.when(z < line - 1)
+            def _():
+                dn_back(low).wait_recv()
+                own[low] = own[low] + dn_in[low].astype(jnp.float32)
+
+            dn_out[low] = own[low].astype(jnp.bfloat16)
+            dn_back(low).start()
+
+        return 0
+
+    lax.fori_loop(0, 2 * (line - 1), back_step, 0)
+    side_back(z).wait_recv()
+    base[...] += own[z] + side_in[z].astype(jnp.float32)
+
+    @pl.when(z > 0)
+    def _():
+        up_back(z).wait_recv()
+        base[...] += up_in[z].astype(jnp.float32)
+
+    @pl.when(z < line - 1)
+    def _():
+        dn_back(z).wait_recv()
+        base[...] += dn_in[z].astype(jnp.float32)
+
+    out_ref[...] = base[...].astype(jnp.bfloat16)
+    for j in range(1, sp_count):
+        gate_move(j).wait_send()
+    for i in range(2):
+        core_copy(i).wait_send()
+    hop.wait_send()
+
+    def drain(where, _):
+        send_side(where).wait_send()
+        side_back(where).wait_send()
+
+        @pl.when(jnp.logical_and(where <= z, z < line - 1))
+        def _():
+            send_up(where).wait_send()
+
+        @pl.when(jnp.logical_and(where >= z, z > 0))
+        def _():
+            send_dn(where).wait_send()
+
+        @pl.when(where > z)
+        def _():
+            up_back(where).wait_send()
+
+        @pl.when(where < z)
+        def _():
+            dn_back(where).wait_send()
+
+        return 0
+
+    lax.fori_loop(0, line, drain, 0)
+
+
+def tail_fused(
+    attended,
+    residual,
+    norm_gain,
+    expert_ids,
+    route_weights,
+    out_weight,
+    expert_gate,
+    expert_up,
+    expert_down,
+    shared_gate,
+    shared_up,
+    shared_down,
+    sp_count,
+):
+    rows, width = residual.shape
+    line = sp_count // 2
+    gates = route_weights / jnp.sum(route_weights, axis=1, keepdims=True) * routed_scale
+    named = expert_ids[None, :, :] == jnp.arange(sp_count, dtype=jnp.int32)[:, None, None]
+    table = jnp.sum(jnp.where(named, gates[None], 0.0), axis=2)
+    lanes = -(-rows // 128) * 128
+    table = jnp.broadcast_to(
+        jnp.pad(table, ((0, 0), (0, lanes - rows)))[:, None, :], (sp_count, 8, lanes)
+    )
+    vmem, hbm = pl.BlockSpec(memory_space=pltpu.VMEM), pl.BlockSpec(memory_space=pl.ANY)
+    bf16, f32 = jnp.bfloat16, jnp.float32
+    loaded = (
+        out_weight,
+        expert_gate[0],
+        expert_up[0],
+        expert_down[0],
+        shared_gate,
+        shared_up,
+        shared_down,
+    )
+    dma = pltpu.SemaphoreType.DMA
+    one = (rows, width)
+    return pl.pallas_call(
+        functools.partial(tail_kernel, sp_count),
+        out_shape=jax.ShapeDtypeStruct(one, bf16),
+        in_specs=[vmem, vmem, vmem] + [hbm] * 8,
+        out_specs=vmem,
+        scratch_shapes=[pltpu.VMEM(w.shape, bf16) for w in loaded]
+        + [
+            pltpu.VMEM(table.shape, f32),
+            pltpu.VMEM(table.shape, f32),
+            pltpu.VMEM((2,) + one, bf16),
+            pltpu.VMEM((2,) + one, bf16),
+            pltpu.VMEM((2,) + one, f32),
+            pltpu.VMEM(one, bf16),
+            pltpu.VMEM(one, bf16),
+            pltpu.VMEM(one, f32),
+            pltpu.VMEM((sp_count,) + one, bf16),
+            pltpu.VMEM((line,) + one, bf16),
+            pltpu.VMEM((line,) + one, bf16),
+            pltpu.VMEM((line,) + one, f32),
+            pltpu.VMEM((line,) + one, bf16),
+            pltpu.VMEM((line,) + one, bf16),
+            pltpu.VMEM((line,) + one, bf16),
+            pltpu.VMEM((line,) + one, bf16),
+            dma((8,)),
+            dma((sp_count - 1,)),
+            dma((sp_count - 1,)),
+            dma((2, 2)),
+            dma((2,)),
+            dma((sp_count,)),
+            dma((2 * line,)),
+            dma((line,)),
+            dma((2 * line,)),
+            dma((line,)),
+            dma((2 * line,)),
+            dma((line,)),
+        ],
+        compiler_params=pltpu.CompilerParams(
+            collective_id=1, has_side_effects=True, vmem_limit_bytes=60 * 2**20
+        ),
+    )(attended, residual, norm_gain[None, :], table, *loaded)
 
 
 def absorb_group(carried, query_group, shard_piece, sum_piece, score_scale):
@@ -88,6 +711,26 @@
     local_kv = key_rows.shape[1] // HEAD_DIM
     group_size = HEADS // KV_HEADS
     score_scale = HEAD_DIM ** (-0.5)
+    tp_count = lax.axis_size("tp")
+    tokens_here = residual.shape[0]
+    every_slot = 2 * tokens_here * TOPK >= tokens_here * expert_gate.shape[0] * sp_count
+    if every_slot and expert_gate.shape[0] == 1 and sp_count % 2 == 0 and tp_count == 4:
+        attended = attend_fused(queries, key_rows, value_rows, forget_sums, sp_count)
+        return tail_fused(
+            attended,
+            residual,
+            norm_gain,
+            expert_ids,
+            route_weights,
+            out_weight,
+            expert_gate,
+            expert_up,
+            expert_down,
+            shared_gate,
+            shared_up,
+            shared_down,
+            sp_count,
+        )
     own_first = sp_index * local_rows
     all_sums = lax.all_gather(forget_sums, "sp", axis=0, tiled=True)
     positions = own_first + jnp.arange(local_rows, dtype=jnp.int32)

time: 272 us -> 129 us (0.47)
  Pallas kernels: 0 us -> 122 us
  waiting for transfers between devices: 118 us -> 0 us
  blocking collectives: 86.7 us -> 0 us
  matrix products: 18.4 us -> 0 us
  local copies, waits for them, and re-layouts: 21.9 us -> 5.04 us
  between operations: 13.3 us -> 0.02 us
  other arithmetic: 6.9 us -> 2.08 us
  starting transfers between devices: 4.77 us -> 0 us
    pallas_call x0 -> x2, Pallas kernels: none -> 122 us  [the longest x1 111 us: tail_fused(): pl.pallas_call(functools.partial(tail_kernel, sp_count), out_shape=jax.Sh...]
    all_to_all x1 -> x0, blocking collectives: 53.7 us -> none  [local(): lax.all_to_all(outgoing, 'sp', split_axis=0, concat_axis=0, tiled=True)]
    all_gather x2 -> x0, waiting for transfers between devices: 45.9 us -> none  [the longest x1 39.2 us: local(): lax.all_gather(value_rows, 'sp', axis=0, tiled=True)]
    all_to_all x1 -> x0, waiting for transfers between devices: 45.2 us -> none  [local(): lax.all_to_all(processed, 'sp', split_axis=0, concat_axis=0, tiled=True)]
    all_gather x1 -> x0, blocking collectives: 33 us -> none  [local(): all_sums = lax.all_gather(forget_sums, 'sp', axis=0, tiled=True)]
    reduce_scatter x1 -> x0, waiting for transfers between devices: 26.4 us -> none  [local(): lax.psum_scatter(jnp.dot(attended, out_weight, preferred_element_type=jnp...]
    dot_general x7 -> x0, matrix products: 18.4 us -> none  [the longest x1 6.24 us: local(): jnp.einsum('necf,efd->necd', hidden, expert_down, preferred_element_type=...]
    gather x2 -> x0, local copies, waits for them, and re-layouts: 7.57 us -> none  [the longest x1 4.22 us: local(): picked = results[target].reshape(rows_out, TOPK, width).astype(jnp.float32)]
  transfers between devices with their start and end apart: 4 -> 0, of which waited for: 4 -> 0; matrix products, arithmetic and copies ran while one was open for 4% -> 0% of each run, Pallas kernels for 0% -> 0%
where the time goes in v1:
time: 129 us
  Pallas kernels  122 us (95%)
  local copies, waits for them, and re-layouts  5.04 us (4%)
  other arithmetic  2.08 us (2%)
    pallas_call x1, Pallas kernels, tail_fused(): pl.pallas_call(functools.partial(tail_kernel, sp_count), out_shape=jax.Sh...  111 us
    pallas_call x1, Pallas kernels, attend_fused(): pl.pallas_call(functools.partial(attend_kernel, sp_count, HEAD_DIM ** (-0...  10.9 us
    unnamed x2, local copies, waits for them, and re-layouts  3.15 us

profile of v1, /device:TPU:0, one launch (start us, length us, event | category | flops | bytes accessed | tf_op | source)
XLA Modules:
  0.0 128.8 jit_solution(14462882695918274091)
XLA Ops:
  0.0 0.7 reduce_sum.18
  0.7 0.7 divide_multiply_fusion
  1.4 0.7 select_reduce_fusion
  2.1 1.3 pad.8.fk_hbm
  3.4 0.6 broadcast_in_dim.28.gate_hbm
  4.0 1.5 %copy.19.fq_ref = f32[256,4]{1,0:T(8,128)} copy(f32[256,4]{0,1:T(4,128)} %param.19) | data formatting | bytes 8192 | tf_op args[4]
  5.5 10.9 %shard_map.145.att_ref = bf16[256,512]{1,0:T(8,128)(2,1)} custom-call(bf16[256,512]{1,0:T(8,128)(2,1)} %q_ref.1, f32[256,4]{1,0:T(8,128)} %copy.19.fq_ref, bf16[256,256]{1,0:T(8,128)(2,1)} %k_hbm.1, bf16[256,256]{1,0:T(8,128)(2,1)} %v_hbm.1, f32[8,256]{1,0:T(8,128)} %pad.8.fk_hbm), custom_call_target="tpu_custom_call" | custom-call | tf_op jit(solution)/shard_map/pallas_call | solution.py:204
  16.4 110.7 %shard_map.146 = bf16[64,2048]{1,0:T(8,128)(2,1)} custom-call(bf16[256,512]{1,0:T(8,128)(2,1)} %shard_map.145.att_ref, bf16[64,2048]{1,0:T(8,128)(2,1)} %res_ref.1, f32[1,2048]{1,0:T(1,128)} %bitcast.9, f32[8,8,128]{2,1,0:T(8,128)} %broadcast_in_dim.28.gate_hbm, bf16[512,2048]{1,0:T(8,128)(2,1)} %wo_hbm.1, bf16[2048,384]{1,0:T(8,128)(2,1)} %bitcast.5, ...), custom_call_target="tpu_custom_call" | custom-call | tf_op jit(solution)/shard_map/pallas_call | solution.py:599
  127.1 1.7 %copy.21 = bf16[64,2048]{1,0:T(8,128)(2,1)} copy(bf16[64,2048]{1,0:T(8,128)(2,1)} %shard_map.146) | data formatting | bytes 524288
  (1 shorter events, 0.0 us)

commit v2 on v1

--- a/solution.py
+++ b/solution.py
@@ -41,15 +41,15 @@
     sp_count,
     score_scale,
     q_ref,
-    fq_ref,
+    f_ref,
     k_hbm,
     v_hbm,
-    fk_hbm,
     out_ref,
     kbuf,
     vbuf,
     fbuf,
     qs,
+    fqs,
     acc,
     top,
     den,
@@ -67,10 +67,12 @@
     bufs = (kbuf, vbuf, fbuf)
     loads = [
         pltpu.make_async_copy(src, buf.at[me], load_sem.at[i])
-        for i, (src, buf) in enumerate(zip((k_hbm, v_hbm, fk_hbm), bufs))
+        for i, (src, buf) in enumerate(zip((k_hbm, v_hbm), bufs))
     ]
     for copy in loads:
         copy.start()
+    fbuf[me] = jnp.zeros(fbuf.shape[1:], jnp.float32)
+    fbuf[me, : f_ref.shape[0], :] = f_ref[...]
     barrier = pltpu.get_barrier_semaphore()
     greet(barrier, mate)
 
@@ -88,6 +90,13 @@
         qs[h // pair, (h % pair) * rows : (h % pair + 1) * rows, :] = q_ref[
             :, h * HEAD_DIM : (h + 1) * HEAD_DIM
         ]
+    square = (rows, rows)
+    diagonal = lax.broadcasted_iota(jnp.int32, square, 0) == lax.broadcasted_iota(jnp.int32, square, 1)
+    for h in range(kv_heads * pair):
+        column = jnp.sum(jnp.where(diagonal, f_ref[h : h + 1, :], 0.0), axis=1, keepdims=True)
+        fqs[h // pair, (h % pair) * rows : (h % pair + 1) * rows, :] = jnp.broadcast_to(
+            column, (rows, HEAD_DIM)
+        )
     for copy in loads:
         copy.wait()
     neighbours = 1 + (z < line - 1).astype(jnp.int32) + (z > 0).astype(jnp.int32)
@@ -99,18 +108,19 @@
             for i, buf in enumerate(bufs)
         ]
 
-    def forward(step):
+    def forward(step, arriving):
         block = 2 * (z - step) + y
-
-        @pl.when(z < line - 1)
-        def _():
-            for copy in moves(block, step, up_sem, above):
-                copy.start()
-
-        @pl.when(jnp.logical_or(y == 0, step > 0))
-        def _():
-            for copy in moves(block, step, side_sem, mate):
-                copy.start()
+        for i in (2, 0, 1):
+            if arriving:
+                moves(block, step, up_sem, below)[i].wait_recv()
+
+            @pl.when(z < line - 1)
+            def _():
+                moves(block, step, up_sem, above)[i].start()
+
+            @pl.when(jnp.logical_or(y == 0, step > 0))
+            def _():
+                moves(block, step, side_sem, mate)[i].start()
 
     def absorb(block, first):
         for g in range(kv_heads):
@@ -122,7 +132,7 @@
             parts = []
             for j in range(pair):
                 h = g * pair + j
-                drop = fq_ref[:, h : h + 1] - fbuf[block, h : h + 1, :]
+                drop = fqs[g, j * rows : (j + 1) * rows, :1] - fbuf[block, h : h + 1, :]
                 part = products[j * rows : (j + 1) * rows] * (score_scale * LOG2E) + drop * LOG2E
                 if first:
                     at_row = lax.broadcasted_iota(jnp.int32, part.shape, 0)
@@ -145,16 +155,14 @@
             top[g] = jnp.broadcast_to(peak, top.shape[1:])
             den[g] = jnp.broadcast_to(total, den.shape[1:])
 
-    forward(0)
+    forward(0, False)
     absorb(me, True)
 
     def one_step(step, _):
         @pl.when(step <= z)
         def _():
             block = 2 * (z - step) + y
-            for copy in moves(block, step, up_sem, below):
-                copy.wait_recv()
-            forward(step)
+            forward(step, True)
             absorb(block, False)
 
         @pl.when(jnp.logical_and(step - 1 <= z, jnp.logical_or(y == 1, step > 1)))
@@ -197,24 +205,24 @@
     rows, width = queries.shape
     kv_heads = key_rows.shape[1] // HEAD_DIM
     heads = width // HEAD_DIM
-    key_sums = jnp.pad(forget_sums.T, ((0, 8 - heads), (0, 0)))
     line = sp_count // 2
     stacked = (kv_heads, heads // kv_heads * rows, HEAD_DIM)
     vmem, hbm = pl.BlockSpec(memory_space=pltpu.VMEM), pl.BlockSpec(memory_space=pl.ANY)
     return pl.pallas_call(
         functools.partial(attend_kernel, sp_count, HEAD_DIM ** (-0.5)),
         out_shape=jax.ShapeDtypeStruct((rows, width), jnp.bfloat16),
-        in_specs=[vmem, vmem, hbm, hbm, hbm],
+        in_specs=[vmem, vmem, hbm, hbm],
         out_specs=vmem,
         scratch_shapes=[
             pltpu.VMEM((sp_count,) + key_rows.shape, jnp.bfloat16),
             pltpu.VMEM((sp_count,) + value_rows.shape, jnp.bfloat16),
-            pltpu.VMEM((sp_count,) + key_sums.shape, jnp.float32),
+            pltpu.VMEM((sp_count, -(-heads // 8) * 8, rows), jnp.float32),
             pltpu.VMEM(stacked, jnp.bfloat16),
             pltpu.VMEM(stacked, jnp.float32),
             pltpu.VMEM(stacked, jnp.float32),
             pltpu.VMEM(stacked, jnp.float32),
-            pltpu.SemaphoreType.DMA((3,)),
+            pltpu.VMEM(stacked, jnp.float32),
+            pltpu.SemaphoreType.DMA((2,)),
             pltpu.SemaphoreType.DMA((line, 3)),
             pltpu.SemaphoreType.DMA((line, 3)),
             pltpu.SemaphoreType.DMA((sp_count, 3)),
@@ -222,7 +230,7 @@
         compiler_params=pltpu.CompilerParams(
             collective_id=0, has_side_effects=True, vmem_limit_bytes=60 * 2**20
         ),
-    )(queries, forget_sums, key_rows, value_rows, key_sums)
+    )(queries, forget_sums.T, key_rows, value_rows)
 
 
 def tail_kernel(
@@ -230,7 +238,8 @@
     att_ref,
     res_ref,
     gain_ref,
-    gate_hbm,
+    ids_ref,
+    score_ref,
     wo_hbm,
     eg_hbm,
     eu_hbm,
@@ -289,7 +298,6 @@
         pltpu.make_async_copy(src, dst, load_sem.at[i])
         for i, (src, dst) in enumerate(
             (
-                (gate_hbm, gate_in),
                 (wo_hbm, wo),
                 (sg_hbm, sg),
                 (su_hbm, su),
@@ -307,8 +315,12 @@
     greet(barrier, x_mate)
     for j in range(1, sp_count):
         greet(barrier, (lax.rem(me + j, sp_count), tp))
+    scores = score_ref[...]
+    gates = scores / jnp.sum(scores, axis=0, keepdims=True) * routed_scale
+    for e in range(sp_count):
+        row = jnp.sum(jnp.where(ids_ref[...] == e, gates, 0.0), axis=0, keepdims=True)
+        gate_in[e] = jnp.broadcast_to(row, gate_in.shape[1:])
     weights[0].wait()
-    weights[1].wait()
     pl.semaphore_wait(barrier, sp_count + 1)
 
     def gate_move(j):
@@ -327,6 +339,11 @@
         gate_move(j).start()
 
     far, near = (1 - x) * 2, x * 2
+
+    def core_copy(i):
+        return remote(core_out.at[i], core_in.at[i], pair_sem.at[0, i], pair_sem.at[1, i], core_mate)
+
+    hop = remote(x_out, x_in, hop_sem.at[0], hop_sem.at[1], x_mate)
 
     def project(block):
         return jnp.dot(
@@ -336,32 +353,22 @@
         )
 
     def project_to(i, _):
-        out_x = jnp.where(i % 2 == 0, far, near)
-
-        @pl.when(i < 2)
+        out_x = jnp.where(i == 0, far, near)
+        core_out[i] = project(out_x + 1 - c).astype(jnp.bfloat16)
+        core_copy(i).start()
+        kept[i] = project(out_x + c)
+        core_copy(i).wait_recv()
+        kept[i] = kept[i] + core_in[i].astype(jnp.float32)
+
+        @pl.when(i == 0)
         def _():
-            core_out[i % 2] = project(out_x + 1 - c).astype(jnp.bfloat16)
-            remote(
-                core_out.at[i % 2], core_in.at[i % 2], pair_sem.at[0, i % 2], pair_sem.at[1, i % 2], core_mate
-            ).start()
-
-        @pl.when(i >= 2)
-        def _():
-            kept[i % 2] = project(out_x + c)
+            x_out[...] = kept[0].astype(jnp.bfloat16)
+            hop.start()
 
         return 0
 
-    lax.fori_loop(0, 4, project_to, 0)
-
-    def core_copy(i):
-        return remote(core_out.at[i], core_in.at[i], pair_sem.at[0, i], pair_sem.at[1, i], core_mate)
-
-    core_copy(0).wait_recv()
-    x_out[...] = (kept[0] + core_in[0].astype(jnp.float32)).astype(jnp.bfloat16)
-    hop = remote(x_out, x_in, hop_sem.at[0], hop_sem.at[1], x_mate)
-    hop.start()
-    core_copy(1).wait_recv()
-    branch = kept[1] + core_in[1].astype(jnp.float32) + res_ref[...].astype(jnp.float32)
+    lax.fori_loop(0, 2, project_to, 0)
+    branch = kept[1] + res_ref[...].astype(jnp.float32)
     hop.wait_recv()
     stream = (branch + x_in[...].astype(jnp.float32)).astype(jnp.bfloat16)
     wide = stream.astype(jnp.float32)
@@ -369,32 +376,39 @@
     tok[me] = (wide * scale * gain_ref[...]).astype(jnp.bfloat16)
     base[...] = wide
 
-    def tok_move(block, sem, target):
-        return remote(tok.at[block], tok.at[block], sem, tok_sem.at[block], target)
+    halves = 2
+    part_rows = rows // halves
+
+    def piece(ref, i, p):
+        return ref.at[i, pl.ds(p * part_rows, part_rows), :]
+
+    def tok_move(block, p, sem, target):
+        return remote(piece(tok, block, p), piece(tok, block, p), sem, tok_sem.at[block, p], target)
 
     def block_of(where):
         return 2 * where + y
 
-    def send_up(where):
-        return tok_move(block_of(where), up_send.at[where], above)
-
-    def send_dn(where):
-        return tok_move(block_of(where), dn_send.at[where], below)
-
-    def send_side(where):
-        return tok_move(block_of(where), side_send.at[where], mate)
-
-    send_side(z).start()
-
-    @pl.when(z < line - 1)
-    def _():
-        send_up(z).start()
-
-    @pl.when(z > 0)
-    def _():
-        send_dn(z).start()
-
-    for copy in weights[2:]:
+    def send_up(where, p):
+        return tok_move(block_of(where), p, up_send.at[where, p], above)
+
+    def send_dn(where, p):
+        return tok_move(block_of(where), p, dn_send.at[where, p], below)
+
+    def send_side(where, p):
+        return tok_move(block_of(where), p, side_send.at[where, p], mate)
+
+    for p in range(halves):
+        send_side(z, p).start()
+
+        @pl.when(z < line - 1)
+        def _():
+            send_up(z, p).start()
+
+        @pl.when(z > 0)
+        def _():
+            send_dn(z, p).start()
+
+    for copy in weights[1:]:
         copy.wait()
 
     def gated(inputs, gate, up, down):
@@ -416,115 +430,163 @@
         result = gated(tok[block], eg, eu, ed).astype(jnp.bfloat16).astype(jnp.float32)
         return result * column
 
-    def side_back(where):
+    def side_back(where, p):
         return remote(
-            side_out.at[where], side_in.at[where], side_send.at[line + where], side_recv.at[where], mate
-        )
+            piece(side_out, where, p),
+            piece(side_in, where, p),
+            side_send.at[line + where, p],
+            side_recv.at[where, p],
+            mate,
+        )
+
+    def inside(where):
+        return jnp.logical_and(where >= 0, where < line)
 
     def mates_block(where):
-        tok_move(2 * where + 1 - y, side_send.at[where], mate).wait_recv()
+        for p in range(halves):
+            tok_move(2 * where + 1 - y, p, side_send.at[where, p], mate).wait_recv()
         side_out[where] = expert(2 * where + 1 - y).astype(jnp.bfloat16)
-        side_back(where).start()
+
+    def own_part(step):
+        def at(i, _):
+            where = jnp.where(i == 0, z - step, z + step)
+
+            @pl.when(inside(where))
+            def _():
+                own[where] = expert(block_of(where))
+
+            return 0
+
+        lax.fori_loop(0, 2, at, 0)
+
+    def mates_part(step):
+        def at(i, _):
+            where = jnp.where(i == 0, z - step, z + step)
+
+            @pl.when(jnp.logical_and(inside(where), jnp.logical_or(i == 0, step > 0)))
+            def _():
+                mates_block(where)
+
+            return 0
+
+        lax.fori_loop(0, 2, at, 0)
 
     own[z] = expert(me)
-    mates_block(z)
 
     def one_step(step, _):
         low, high = z - step, z + step
-
-        @pl.when(low >= 0)
+        for p in range(halves):
+
+            @pl.when(low >= 0)
+            def _():
+                tok_move(block_of(low), p, up_send.at[low, p], below).wait_recv()
+                send_side(low, p).start()
+
+                @pl.when(z < line - 1)
+                def _():
+                    send_up(low, p).start()
+
+            @pl.when(high < line)
+            def _():
+                tok_move(block_of(high), p, dn_send.at[high, p], above).wait_recv()
+                send_side(high, p).start()
+
+                @pl.when(z > 0)
+                def _():
+                    send_dn(high, p).start()
+
+        @pl.when(step == line - 1)
         def _():
-            tok_move(block_of(low), up_send.at[low], below).wait_recv()
-            send_side(low).start()
-
-            @pl.when(z < line - 1)
-            def _():
-                send_up(low).start()
-
-        @pl.when(high < line)
-        def _():
-            tok_move(block_of(high), dn_send.at[high], above).wait_recv()
-            send_side(high).start()
-
-            @pl.when(z > 0)
-            def _():
-                send_dn(high).start()
-
-        def at(i, _):
-            where = jnp.where(i == 0, low, high)
-
-            @pl.when(jnp.logical_and(where >= 0, where < line))
-            def _():
-                own[where] = expert(block_of(where))
-
-            return 0
-
-        def at_mates(i, _):
-            where = jnp.where(i == 0, low, high)
-
-            @pl.when(jnp.logical_and(where >= 0, where < line))
-            def _():
-                mates_block(where)
-
-            return 0
-
-        lax.fori_loop(0, 2, at, 0)
-        lax.fori_loop(0, 2, at_mates, 0)
+            for p in range(halves):
+                side_back(z, p).start()
+
+        own_part(step)
+        mates_part(step - 1)
         return 0
 
     lax.fori_loop(1, line, one_step, 0)
-
-    def up_back(where):
-        return remote(up_out.at[where], up_in.at[where], up_send.at[line + where], up_recv.at[where], above)
-
-    def dn_back(where):
-        return remote(dn_out.at[where], dn_in.at[where], dn_send.at[line + where], dn_recv.at[where], below)
+    mates_part(line - 1)
+
+    def cross(turn, _):
+        step = line - 1 - turn
+        for where in (z - step, z + step):
+
+            @pl.when(inside(where))
+            def _():
+                for p in range(halves):
+                    side_back(where, p).start()
+
+        return 0
+
+    lax.fori_loop(0, line - 1, cross, 0)
+
+    def up_back(where, p):
+        return remote(
+            piece(up_out, where, p),
+            piece(up_in, where, p),
+            up_send.at[line + where, p],
+            up_recv.at[where, p],
+            above,
+        )
+
+    def dn_back(where, p):
+        return remote(
+            piece(dn_out, where, p),
+            piece(dn_in, where, p),
+            dn_send.at[line + where, p],
+            dn_recv.at[where, p],
+            below,
+        )
 
     def back_step(turn, _):
-        step = turn % (line - 1) + 1
+        step = line - 1 - turn % (line - 1)
         upward = (turn < line - 1) == (2 * z < line - 1)
         low, high = z - step, z + step
 
+        def pass_on(where, chained, back, came, leaving):
+            for p in range(halves):
+                span = pl.ds(p * part_rows, part_rows)
+                side_back(where, p).wait_recv()
+                leaving[where, span, :] = (
+                    own[where, span, :] + side_in[where, span, :].astype(jnp.float32)
+                ).astype(jnp.bfloat16)
+
+                @pl.when(chained)
+                def _():
+                    back(where, p).wait_recv()
+                    leaving[where, span, :] = (
+                        own[where, span, :]
+                        + side_in[where, span, :].astype(jnp.float32)
+                        + came[where, span, :].astype(jnp.float32)
+                    ).astype(jnp.bfloat16)
+
+                back(where, p).start()
+
         @pl.when(jnp.logical_and(upward, high < line))
         def _():
-            side_back(high).wait_recv()
-            own[high] = own[high] + side_in[high].astype(jnp.float32)
-
-            @pl.when(z > 0)
-            def _():
-                up_back(high).wait_recv()
-                own[high] = own[high] + up_in[high].astype(jnp.float32)
-
-            up_out[high] = own[high].astype(jnp.bfloat16)
-            up_back(high).start()
+            pass_on(high, z > 0, up_back, up_in, up_out)
 
         @pl.when(jnp.logical_and(jnp.logical_not(upward), low >= 0))
         def _():
-            side_back(low).wait_recv()
-            own[low] = own[low] + side_in[low].astype(jnp.float32)
-
-            @pl.when(z < line - 1)
-            def _():
-                dn_back(low).wait_recv()
-                own[low] = own[low] + dn_in[low].astype(jnp.float32)
-
-            dn_out[low] = own[low].astype(jnp.bfloat16)
-            dn_back(low).start()
+            pass_on(low, z < line - 1, dn_back, dn_in, dn_out)
 
         return 0
 
     lax.fori_loop(0, 2 * (line - 1), back_step, 0)
-    side_back(z).wait_recv()
+    for p in range(halves):
+        side_back(z, p).wait_recv()
     base[...] += own[z] + side_in[z].astype(jnp.float32)
 
     @pl.when(z > 0)
     def _():
-        up_back(z).wait_recv()
+        for p in range(halves):
+            up_back(z, p).wait_recv()
         base[...] += up_in[z].astype(jnp.float32)
 
     @pl.when(z < line - 1)
     def _():
-        dn_back(z).wait_recv()
+        for p in range(halves):
+            dn_back(z, p).wait_recv()
         base[...] += dn_in[z].astype(jnp.float32)
 
     out_ref[...] = base[...].astype(jnp.bfloat16)
@@ -535,24 +597,25 @@
     hop.wait_send()
 
     def drain(where, _):
-        send_side(where).wait_send()
-        side_back(where).wait_send()
-
-        @pl.when(jnp.logical_and(where <= z, z < line - 1))
-        def _():
-            send_up(where).wait_send()
-
-        @pl.when(jnp.logical_and(where >= z, z > 0))
-        def _():
-            send_dn(where).wait_send()
-
-        @pl.when(where > z)
-        def _():
-            up_back(where).wait_send()
-
-        @pl.when(where < z)
-        def _():
-            dn_back(where).wait_send()
+        for p in range(halves):
+            send_side(where, p).wait_send()
+            side_back(where, p).wait_send()
+
+            @pl.when(jnp.logical_and(where <= z, z < line - 1))
+            def _():
+                send_up(where, p).wait_send()
+
+            @pl.when(jnp.logical_and(where >= z, z > 0))
+            def _():
+                send_dn(where, p).wait_send()
+
+            @pl.when(where > z)
+            def _():
+                up_back(where, p).wait_send()
+
+            @pl.when(where < z)
+            def _():
+                dn_back(where, p).wait_send()
 
         return 0
 
@@ -576,13 +639,7 @@
 ):
     rows, width = residual.shape
     line = sp_count // 2
-    gates = route_weights / jnp.sum(route_weights, axis=1, keepdims=True) * routed_scale
-    named = expert_ids[None, :, :] == jnp.arange(sp_count, dtype=jnp.int32)[:, None, None]
-    table = jnp.sum(jnp.where(named, gates[None], 0.0), axis=2)
-    lanes = -(-rows // 128) * 128
-    table = jnp.broadcast_to(
-        jnp.pad(table, ((0, 0), (0, lanes - rows)))[:, None, :], (sp_count, 8, lanes)
-    )
+    table = (sp_count, 8, rows)
     vmem, hbm = pl.BlockSpec(memory_space=pltpu.VMEM), pl.BlockSpec(memory_space=pl.ANY)
     bf16, f32 = jnp.bfloat16, jnp.float32
     loaded = (
@@ -599,12 +656,12 @@
     return pl.pallas_call(
         functools.partial(tail_kernel, sp_count),
         out_shape=jax.ShapeDtypeStruct(one, bf16),
-        in_specs=[vmem, vmem, vmem] + [hbm] * 8,
+        in_specs=[vmem] * 5 + [hbm] * 7,
         out_specs=vmem,
         scratch_shapes=[pltpu.VMEM(w.shape, bf16) for w in loaded]
         + [
-            pltpu.VMEM(table.shape, f32),
-            pltpu.VMEM(table.shape, f32),
+            pltpu.VMEM(table, f32),
+            pltpu.VMEM(table, f32),
             pltpu.VMEM((2,) + one, bf16),
             pltpu.VMEM((2,) + one, bf16),
             pltpu.VMEM((2,) + one, f32),
@@ -619,23 +676,23 @@
             pltpu.VMEM((line,) + one, bf16),
             pltpu.VMEM((line,) + one, bf16),
             pltpu.VMEM((line,) + one, bf16),
-            dma((8,)),
+            dma((7,)),
             dma((sp_count - 1,)),
             dma((sp_count - 1,)),
             dma((2, 2)),
             dma((2,)),
-            dma((sp_count,)),
-            dma((2 * line,)),
-            dma((line,)),
-            dma((2 * line,)),
-            dma((line,)),
-            dma((2 * line,)),
-            dma((line,)),
+            dma((sp_count, 2)),
+            dma((2 * line, 2)),
+            dma((line, 2)),
+            dma((2 * line, 2)),
+            dma((line, 2)),
+            dma((2 * line, 2)),
+            dma((line, 2)),
         ],
         compiler_params=pltpu.CompilerParams(
             collective_id=1, has_side_effects=True, vmem_limit_bytes=60 * 2**20
         ),
-    )(attended, residual, norm_gain[None, :], table, *loaded)
+    )(attended, residual, norm_gain[None, :], expert_ids.T, route_weights.T, *loaded)
 
 
 def absorb_group(carried, query_group, shard_piece, sum_piece, score_scale):
@@ -714,7 +771,7 @@
     tp_count = lax.axis_size("tp")
     tokens_here = residual.shape[0]
     every_slot = 2 * tokens_here * TOPK >= tokens_here * expert_gate.shape[0] * sp_count
-    if every_slot and expert_gate.shape[0] == 1 and sp_count % 2 == 0 and tp_count == 4:
+    if every_slot and expert_gate.shape[0] == 1 and sp_count % 2 == 0 and sp_count > 4 and tp_count == 4:
         attended = attend_fused(queries, key_rows, value_rows, forget_sums, sp_count)
         return tail_fused(
             attended,

time: 129 us -> 104 us (0.81)
  Pallas kernels: 122 us -> 102 us
  local copies, waits for them, and re-layouts: 5.04 us -> 1.67 us
  other arithmetic: 2.08 us -> 0 us
    pallas_call x1, Pallas kernels: 111 us -> 91 us  [tail_fused(): pl.pallas_call(functools.partial(tail_kernel, sp_count), out_shape=jax.Sh...]
    unnamed x2 -> x1, local copies, waits for them, and re-layouts: 3.15 us -> 1.67 us
    reduce_sum x2 -> x0, other arithmetic: 1.39 us -> none  [the longest x1 0.7 us: tail_fused(): jnp.sum(route_weights, axis=1, keepdims=True)]
where the time goes in v2:
time: 104 us
  Pallas kernels  102 us (98%)
  local copies, waits for them, and re-layouts  1.67 us (2%)
    pallas_call x1, Pallas kernels, tail_fused(): pl.pallas_call(functools.partial(tail_kernel, sp_count), out_shape=jax.Sh...  91 us
    pallas_call x1, Pallas kernels, attend_fused(): pl.pallas_call(functools.partial(attend_kernel, sp_count, HEAD_DIM ** (-0...  10.9 us

profile of v2, /device:TPU:0, one launch (start us, length us, event | category | flops | bytes accessed | tf_op | source)
XLA Modules:
  0.0 103.6 jit_solution(676482675088598181)
XLA Ops:
  0.0 10.9 %shard_map.145.att_ref = bf16[256,512]{1,0:T(8,128)(2,1)} custom-call(bf16[256,512]{1,0:T(8,128)(2,1)} %q_ref.1, f32[4,256]{1,0:T(4,128)} %bitcast.11, bf16[256,256]{1,0:T(8,128)(2,1)} %k_hbm.1, bf16[256,256]{1,0:T(8,128)(2,1)} %v_hbm.1), custom_call_target="tpu_custom_call" | custom-call | tf_op jit(solution)/shard_map/pallas_call | solution.py:211
  10.9 91.0 %shard_map.146 = bf16[64,2048]{1,0:T(8,128)(2,1)} custom-call(bf16[256,512]{1,0:T(8,128)(2,1)} %shard_map.145.att_ref, bf16[64,2048]{1,0:T(8,128)(2,1)} %res_ref.1, f32[1,2048]{1,0:T(1,128)} %bitcast.10, s32[4,64]{1,0:T(4,128)} %bitcast.12, f32[4,64]{1,0:T(4,128)} %bitcast.13, bf16[512,2048]{1,0:T(8,128)(2,1)} %wo_hbm.1, bf16[2048,384]{1,0:T(8,128)(2,1)} %bitcast.7, ...), custom_call_target="tpu_custom_call" | custom-call | tf_op jit(solution)/shard_map/pallas_call | solution.py:656
  102.0 1.7 %copy.17 = bf16[64,2048]{1,0:T(8,128)(2,1)} copy(bf16[64,2048]{1,0:T(8,128)(2,1)} %shard_map.146) | data formatting | bytes 524288

commit v3 on v2

--- a/solution.py
+++ b/solution.py
@@ -38,6 +38,7 @@
 
 
 def attend_kernel(
+    enter,
     sp_count,
     score_scale,
     q_ref,
@@ -73,17 +74,6 @@
         copy.start()
     fbuf[me] = jnp.zeros(fbuf.shape[1:], jnp.float32)
     fbuf[me, : f_ref.shape[0], :] = f_ref[...]
-    barrier = pltpu.get_barrier_semaphore()
-    greet(barrier, mate)
-
-    @pl.when(z < line - 1)
-    def _():
-        greet(barrier, above)
-
-    @pl.when(z > 0)
-    def _():
-        greet(barrier, below)
-
     rows, pair = q_ref.shape[0], qs.shape[1] // q_ref.shape[0]
     kv_heads = qs.shape[0]
     for h in range(kv_heads * pair):
@@ -99,8 +89,7 @@
         )
     for copy in loads:
         copy.wait()
-    neighbours = 1 + (z < line - 1).astype(jnp.int32) + (z > 0).astype(jnp.int32)
-    pl.semaphore_wait(barrier, neighbours)
+    enter()
 
     def moves(block, step, sems, target):
         return [
@@ -201,39 +190,8 @@
     lax.fori_loop(0, line, drain, 0)
 
 
-def attend_fused(queries, key_rows, value_rows, forget_sums, sp_count):
-    rows, width = queries.shape
-    kv_heads = key_rows.shape[1] // HEAD_DIM
-    heads = width // HEAD_DIM
-    line = sp_count // 2
-    stacked = (kv_heads, heads // kv_heads * rows, HEAD_DIM)
-    vmem, hbm = pl.BlockSpec(memory_space=pltpu.VMEM), pl.BlockSpec(memory_space=pl.ANY)
-    return pl.pallas_call(
-        functools.partial(attend_kernel, sp_count, HEAD_DIM ** (-0.5)),
-        out_shape=jax.ShapeDtypeStruct((rows, width), jnp.bfloat16),
-        in_specs=[vmem, vmem, hbm, hbm],
-        out_specs=vmem,
-        scratch_shapes=[
-            pltpu.VMEM((sp_count,) + key_rows.shape, jnp.bfloat16),
-            pltpu.VMEM((sp_count,) + value_rows.shape, jnp.bfloat16),
-            pltpu.VMEM((sp_count, -(-heads // 8) * 8, rows), jnp.float32),
-            pltpu.VMEM(stacked, jnp.bfloat16),
-            pltpu.VMEM(stacked, jnp.float32),
-            pltpu.VMEM(stacked, jnp.float32),
-            pltpu.VMEM(stacked, jnp.float32),
-            pltpu.VMEM(stacked, jnp.float32),
-            pltpu.SemaphoreType.DMA((2,)),
-            pltpu.SemaphoreType.DMA((line, 3)),
-            pltpu.SemaphoreType.DMA((line, 3)),
-            pltpu.SemaphoreType.DMA((sp_count, 3)),
-        ],
-        compiler_params=pltpu.CompilerParams(
-            collective_id=0, has_side_effects=True, vmem_limit_bytes=60 * 2**20
-        ),
-    )(queries, forget_sums.T, key_rows, value_rows)
-
-
 def tail_kernel(
+    weights,
     sp_count,
     att_ref,
     res_ref,
@@ -294,34 +252,12 @@
     core_mate = (me, 2 * x + 1 - c)
     x_mate = (me, 2 * (1 - x) + c)
     rows = res_ref.shape[0]
-    weights = [
-        pltpu.make_async_copy(src, dst, load_sem.at[i])
-        for i, (src, dst) in enumerate(
-            (
-                (wo_hbm, wo),
-                (sg_hbm, sg),
-                (su_hbm, su),
-                (sd_hbm, sd),
-                (eg_hbm, eg),
-                (eu_hbm, eu),
-                (ed_hbm, ed),
-            )
-        )
-    ]
-    for copy in weights:
-        copy.start()
-    barrier = pltpu.get_barrier_semaphore()
-    greet(barrier, core_mate)
-    greet(barrier, x_mate)
-    for j in range(1, sp_count):
-        greet(barrier, (lax.rem(me + j, sp_count), tp))
     scores = score_ref[...]
     gates = scores / jnp.sum(scores, axis=0, keepdims=True) * routed_scale
     for e in range(sp_count):
         row = jnp.sum(jnp.where(ids_ref[...] == e, gates, 0.0), axis=0, keepdims=True)
         gate_in[e] = jnp.broadcast_to(row, gate_in.shape[1:])
     weights[0].wait()
-    pl.semaphore_wait(barrier, sp_count + 1)
 
     def gate_move(j):
         peer, source = lax.rem(me + j, sp_count), me
@@ -622,9 +558,39 @@
     lax.fori_loop(0, line, drain, 0)
 
 
-def tail_fused(
-    attended,
+def layer_kernel(sp_count, score_scale, q_ref, f_ref, k_hbm, v_hbm, res_ref, gain_ref, ids_ref, score_ref, *rest):
+    sources, out_ref, rest = rest[:7], rest[7], rest[8:]
+    att_ref, attend_scratch, tail_scratch = rest[0], rest[1:13], rest[13:]
+    load_sem = tail_scratch[23]
+    me, tp = lax.axis_index("sp"), lax.axis_index("tp")
+    x, c = tp // 2, tp % 2
+    held = tail_scratch[:7]
+    weights = [
+        pltpu.make_async_copy(sources[i], held[i], load_sem.at[i]) for i in (0, 4, 5, 6, 1, 2, 3)
+    ]
+    barrier = pltpu.get_barrier_semaphore()
+    greet(barrier, (me, 2 * x + 1 - c))
+    greet(barrier, (me, 2 * (1 - x) + c))
+    for j in range(1, sp_count):
+        greet(barrier, (lax.rem(me + j, sp_count), tp))
+
+    def enter():
+        pl.semaphore_wait(barrier, sp_count + 1)
+        for copy in weights:
+            copy.start()
+
+    attend_kernel(enter, sp_count, score_scale, q_ref, f_ref, k_hbm, v_hbm, att_ref, *attend_scratch)
+    tail_kernel(
+        weights, sp_count, att_ref, res_ref, gain_ref, ids_ref, score_ref, *sources, out_ref, *tail_scratch
+    )
+
+
+def layer_fused(
     residual,
+    queries,
+    key_rows,
+    value_rows,
+    forget_sums,
     norm_gain,
     expert_ids,
     route_weights,
@@ -637,6 +603,9 @@
     shared_down,
     sp_count,
 ):
+    query_rows, heads = queries.shape[0], forget_sums.shape[1]
+    kv_heads = key_rows.shape[1] // HEAD_DIM
+    stacked = (kv_heads, heads // kv_heads * query_rows, HEAD_DIM)
     rows, width = residual.shape
     line = sp_count // 2
     table = (sp_count, 8, rows)
@@ -654,11 +623,26 @@
     dma = pltpu.SemaphoreType.DMA
     one = (rows, width)
     return pl.pallas_call(
-        functools.partial(tail_kernel, sp_count),
+        functools.partial(layer_kernel, sp_count, HEAD_DIM ** (-0.5)),
         out_shape=jax.ShapeDtypeStruct(one, bf16),
-        in_specs=[vmem] * 5 + [hbm] * 7,
+        in_specs=[vmem, vmem, hbm, hbm] + [vmem] * 4 + [hbm] * 7,
         out_specs=vmem,
-        scratch_shapes=[pltpu.VMEM(w.shape, bf16) for w in loaded]
+        scratch_shapes=[
+            pltpu.VMEM(queries.shape, bf16),
+            pltpu.VMEM((sp_count,) + key_rows.shape, bf16),
+            pltpu.VMEM((sp_count,) + value_rows.shape, bf16),
+            pltpu.VMEM((sp_count, -(-heads // 8) * 8, query_rows), f32),
+            pltpu.VMEM(stacked, bf16),
+            pltpu.VMEM(stacked, f32),
+            pltpu.VMEM(stacked, f32),
+            pltpu.VMEM(stacked, f32),
+            pltpu.VMEM(stacked, f32),
+            dma((2,)),
+            dma((line, 3)),
+            dma((line, 3)),
+            dma((sp_count, 3)),
+        ]
+        + [pltpu.VMEM(w.shape, bf16) for w in loaded]
         + [
             pltpu.VMEM(table, f32),
             pltpu.VMEM(table, f32),
@@ -690,9 +674,19 @@
             dma((line, 2)),
         ],
         compiler_params=pltpu.CompilerParams(
-            collective_id=1, has_side_effects=True, vmem_limit_bytes=60 * 2**20
+            collective_id=0, has_side_effects=True, vmem_limit_bytes=60 * 2**20
         ),
-    )(attended, residual, norm_gain[None, :], expert_ids.T, route_weights.T, *loaded)
+    )(
+        queries,
+        forget_sums.T,
+        key_rows,
+        value_rows,
+        residual,
+        norm_gain[None, :],
+        expert_ids.T,
+        route_weights.T,
+        *loaded,
+    )
 
 
 def absorb_group(carried, query_group, shard_piece, sum_piece, score_scale):
@@ -772,10 +766,12 @@
     tokens_here = residual.shape[0]
     every_slot = 2 * tokens_here * TOPK >= tokens_here * expert_gate.shape[0] * sp_count
     if every_slot and expert_gate.shape[0] == 1 and sp_count % 2 == 0 and sp_count > 4 and tp_count == 4:
-        attended = attend_fused(queries, key_rows, value_rows, forget_sums, sp_count)
-        return tail_fused(
-            attended,
+        return layer_fused(
             residual,
+            queries,
+            key_rows,
+            value_rows,
+            forget_sums,
             norm_gain,
             expert_ids,
             route_weights,

time: 104 us -> 96.8 us (0.931)
  Pallas kernels: 102 us -> 94.5 us
    pallas_call x2 -> x1, Pallas kernels: 102 us -> 94.5 us  [layer_fused(): pl.pallas_call(functools.partial(layer_kernel, sp_count, HEAD_DIM ** (-0....]
where the time goes in v3:
time: 96.8 us; the launch traced here: 96.2 us
  Pallas kernels  94.5 us (98%)
  local copies, waits for them, and re-layouts  1.67 us (2%)
    pallas_call x1, Pallas kernels, layer_fused(): pl.pallas_call(functools.partial(layer_kernel, sp_count, HEAD_DIM ** (-0....  94.5 us

profile of v3, /device:TPU:0, one launch (start us, length us, event | category | flops | bytes accessed | tf_op | source)
XLA Modules:
  0.0 96.2 jit_solution(13948936968205842023)
XLA Ops:
  0.0 94.5 %shard_map.145 = bf16[64,2048]{1,0:T(8,128)(2,1)} custom-call(bf16[256,512]{1,0:T(8,128)(2,1)} %q_ref.1, f32[4,256]{1,0:T(4,128)} %bitcast.11, bf16[256,256]{1,0:T(8,128)(2,1)} %k_hbm.1, bf16[256,256]{1,0:T(8,128)(2,1)} %v_hbm.1, bf16[64,2048]{1,0:T(8,128)(2,1)} %res_ref.1, f32[1,2048]{1,0:T(1,128)} %bitcast.10, s32[4,64]{1,0:T(4,128)} %bitcast.12, ...), custom_call_target="tpu_custom_call" | custom-call | tf_op jit(solution)/shard_map/pallas_call | solution.py:625
  94.5 1.7 %copy.17 = bf16[64,2048]{1,0:T(8,128)(2,1)} copy(bf16[64,2048]{1,0:T(8,128)(2,1)} %shard_map.145) | data formatting | bytes 524288
